TPU v7x, 32 devices: a whole 2x2x4 slice. The times are simulated.
32 devices in a mesh: fs: 16 (over z, y, x), tp: 2 (over core).
Axes of the slice: x: 2, y: 2, z: 4, core: 2. Of those that a mesh axis runs over, the one named last changes fastest.
Arguments:
- normed_input: bfloat16 [8192, 4096], P('fs', 'tp'), may hold values from -6 to 6
- value_cotangent: bfloat16 [8192, 2048], P('fs', 'tp'), may hold values from -0.01171875 to 0.01171875
- mixer_output: bfloat16 [8192, 2048], P('fs', 'tp'), may hold values from -6 to 6
- output_cotangent: bfloat16 [8192, 4096], P('fs', 'tp'), may hold values from -0.015625 to 0.015625
- value_factor: bfloat16 [4096, 128], replicated, may hold values from -0.5 to 0.5
- output_factor: bfloat16 [2048, 128], replicated, may hold values from -0.5 to 0.5
- value_master: float32 [4096, 2048], P('fs', 'tp'), may hold values from -0.09375 to 0.09375
- value_moment: float32 [128, 2048], P(None, 'tp'), may hold values from -6 to 6
- value_second: float32 [128, 2048], P(None, 'tp'), may hold values from 0.0625 to 16, as said below
- output_master: float32 [2048, 4096], P('fs', 'tp'), may hold values from -0.125 to 0.125
- output_moment: float32 [128, 4096], P(None, 'tp'), may hold values from -6 to 6
- output_second: float32 [128, 4096], P(None, 'tp'), may hold values from 0.0625 to 16, as said below
Outputs:
- value_step: float32 [4096, 2048], P('fs', 'tp')
- value_new: float32 [4096, 2048], P('fs', 'tp')
- value_copy: bfloat16 [4096, 2048], P(None, 'tp')
- value_moment_new: float32 [128, 2048], P(None, 'tp')
- value_second_new: float32 [128, 2048], P(None, 'tp')
- output_step: float32 [2048, 4096], P('fs', 'tp')
- output_new: float32 [2048, 4096], P('fs', 'tp')
- output_copy: bfloat16 [2048, 4096], P(None, 'tp')
- output_moment_new: float32 [128, 4096], P(None, 'tp')
- output_second_new: float32 [128, 4096], P(None, 'tp')
Inputs may be any that keep to these rules, and one draw needn't show every extreme that they name: `value_second`: positive, with a scale that differs between groups of columns. `output_second`: positive, with a scale that differs between groups of columns.
All inputs are finite; a program needn't handle non-finite values.
Results may differ from a plain program's by a relative error of at most 0.004.
Values may be sent and summed in bfloat16 or wider, within the bound.
A program may use at most 128 MiB of HBM per device.

v0:
```python
import jax
import jax.numpy as jnp
from jax import lax
from jax.sharding import PartitionSpec as P

D = 4096
WIDTH = 2048
R = 128


BETA_ONE = 0.8
BETA_TWO = 0.9
EPSILON = 1e-08
STEP_RATE = 0.005
FLOOR = 0.25


def contract_rows(left, right):
    return lax.dot_general(
        left.astype(jnp.float32),
        right.astype(jnp.float32),
        (((0,), (0,)), ((), ())),
        preferred_element_type=jnp.float32,
        precision=lax.Precision.HIGHEST,
    )


def moments(first, second, projected):
    first_new = BETA_ONE * first + (1.0 - BETA_ONE) * projected
    second_new = BETA_TWO * second + (1.0 - BETA_TWO) * projected * projected
    normalized = first_new / (jnp.sqrt(second_new) + EPSILON)
    return (first_new, second_new, normalized)


def per_device(
    normed_input,
    value_cotangent,
    mixer_output,
    output_cotangent,
    value_factor,
    output_factor,
    value_master,
    value_moment,
    value_second,
    output_master,
    output_moment,
    output_second,
):
    highest = lax.Precision.HIGHEST
    row_index = lax.axis_index("fs")
    column_index = lax.axis_index("tp")
    value_rows = value_master.shape[0]
    output_rows = output_master.shape[0]
    factor_here = lax.dynamic_slice_in_dim(
        value_factor, row_index * value_rows, value_rows, 0
    ).astype(jnp.float32)
    feature_cols = normed_input.shape[1]
    factor_features = lax.dynamic_slice_in_dim(
        value_factor, column_index * feature_cols, feature_cols, 0
    )
    input_partial = jnp.dot(normed_input, factor_features, preferred_element_type=jnp.float32)
    input_reduced = lax.psum(input_partial.astype(jnp.bfloat16), "tp").astype(jnp.float32)
    value_partial = contract_rows(input_reduced, value_cotangent)
    head_cols = mixer_output.shape[1]
    factor_heads = lax.dynamic_slice_in_dim(output_factor, column_index * head_cols, head_cols, 0)
    mixer_partial = jnp.dot(mixer_output, factor_heads, preferred_element_type=jnp.float32).astype(
        jnp.bfloat16
    )
    mixer_partial = lax.optimization_barrier(mixer_partial)
    mixer_reduced = lax.psum(mixer_partial.astype(jnp.float32).astype(jnp.bfloat16), "tp")
    output_partial = contract_rows(mixer_reduced, output_cotangent)
    value_projected, output_projected = lax.psum((value_partial, output_partial), "fs")
    value_moment_new, value_second_new, value_norm = moments(
        value_moment, value_second, value_projected
    )
    output_moment_new, output_second_new, output_norm = moments(
        output_moment, output_second, output_projected
    )
    value_total, output_total = lax.psum(
        (jnp.sum(value_norm * value_norm), jnp.sum(output_norm * output_norm)), "tp"
    )
    value_scale = lax.rsqrt(value_total / (R * WIDTH) + FLOOR)
    output_scale = lax.rsqrt(output_total / (R * D) + FLOOR)
    value_step = value_scale * jnp.dot(factor_here, value_norm, precision=highest)
    output_factor_rows = lax.dynamic_slice_in_dim(
        output_factor, row_index * output_rows, output_rows, 0
    ).astype(jnp.float32)
    output_step = output_scale * jnp.dot(output_factor_rows, output_norm, precision=highest)
    value_new = value_master - STEP_RATE * value_step
    output_new = output_master - STEP_RATE * output_step
    value_copy, output_copy = (
        lax.all_gather(value_new.astype(jnp.bfloat16), "fs", axis=0, tiled=True),
        lax.all_gather(output_new.astype(jnp.bfloat16), "fs", axis=0, tiled=True),
    )
    return (
        value_step,
        value_new,
        value_copy,
        value_moment_new,
        value_second_new,
        output_step,
        output_new,
        output_copy,
        output_moment_new,
        output_second_new,
    )


def solution(mesh):
    return jax.shard_map(
        per_device,
        mesh=mesh,
        in_specs=(
            P("fs", "tp"),
            P("fs", "tp"),
            P("fs", "tp"),
            P("fs", "tp"),
            P(),
            P(),
            P("fs", "tp"),
            P(None, "tp"),
            P(None, "tp"),
            P("fs", "tp"),
            P(None, "tp"),
            P(None, "tp"),
        ),
        out_specs=(
            P("fs", "tp"),
            P("fs", "tp"),
            P(None, "tp"),
            P(None, "tp"),
            P(None, "tp"),
            P("fs", "tp"),
            P("fs", "tp"),
            P(None, "tp"),
            P(None, "tp"),
            P(None, "tp"),
        ),
        check_vma=False,
    )
```

profile of v0, /device:TPU:0, one launch (start us, length us, event | category | flops | bytes accessed | tf_op | source)
XLA Modules:
  0.0 422.5 jit_solution(4155375352254664596)
XLA Ops:
  7.2 0.0 copy-start
  7.2 0.0 all-reduce.8.cloned.1.call-start
  7.2 0.0 copy-start.2
  7.3 2.6 fusion.1
  9.9 3.3 fusion
  13.1 0.0 all-reduce.8.cloned.1.call-update
  13.1 0.0 all-reduce.6.cloned.1.call-start
  13.2 21.1 %all-reduce.8.cloned.1.call-done = (bf16[512,128]{0,1:T(8,128)(2,1)}, bf16[512,128]{0,1:T(8,128)(2,1)}) async-done(((bf16[512,128]{0,1:T(8,128)(2,1)}, bf16[512,128]{0,1:T(8,128)(2,1)}), (bf16[512,128]{0,1:T(8,128)(2,1)}, bf16[512,128]{0,1:T(8,128)(2,1)})) %all-reduce.8.cloned.1.call-update) | async-done | bytes 262160 | tf_op jit(solution)/shard_map/psum | solution.py:62
  34.3 0.0 copy-done.2
  34.3 2.0 fusion.16
  36.3 0.0 copy-done
  36.3 0.0 copy-start.4
  36.3 2.4 fusion.17
  38.7 0.0 all-reduce.6.cloned.1.call-update
  38.8 0.0 all-gather.3.cloned.1.call-start
  38.8 121.2 %all-reduce.6.cloned.1.call-done = (f32[128,1024]{1,0:T(8,128)}, f32[128,2048]{1,0:T(8,128)}) async-done(((f32[128,1024]{1,0:T(8,128)}, f32[128,2048]{1,0:T(8,128)}), (f32[128,1024]{1,0:T(8,128)}, f32[128,2048]{1,0:T(8,128)})) %all-reduce.6.cloned.1.call-update) | async-done | bytes 1572880 | tf_op jit(solution)/shard_map/psum | solution.py:72
  160.0 0.0 copy-done.4
  160.0 0.0 copy-done.5
  160.0 3.0 multiply_reduce_fusion.1
  163.0 0.0 copy-done.3
  163.0 3.7 multiply_reduce_fusion
  166.8 3.1 all-reduce.1
  170.6 3.9 fusion.13
  174.4 0.0 all-gather.3.cloned.1.call-update
  174.5 0.0 all-gather.5.cloned.1.call-start
  175.2 0.0 copy-done.1
  175.2 4.2 fusion.12
  179.4 0.0 all-gather.5.cloned.1.call-update
  179.4 106.7 %all-gather.3.cloned.1.call-done = bf16[4096,1024]{1,0:T(8,128)(2,1)} async-done(((bf16[256,1024]{1,0:T(8,128)(2,1)}), bf16[4096,1024]{1,0:T(8,128)(2,1)}) %all-gather.3.cloned.1.call-update) | async-done | bytes 8388624 | tf_op jit(solution)/shard_map/all_gather | solution.py:92
  286.1 113.7 %all-gather.5.cloned.1.call-done = bf16[2048,2048]{1,0:T(8,128)(2,1)} async-done(((bf16[128,2048]{1,0:T(8,128)(2,1)}), bf16[2048,2048]{1,0:T(8,128)(2,1)}) %all-gather.5.cloned.1.call-update) | async-done | bytes 8388624 | tf_op jit(solution)/shard_map/all_gather | solution.py:93
  399.8 7.8 %copy.28 = bf16[4096,1024]{1,0:T(8,128)(2,1)} copy(bf16[4096,1024]{1,0:T(8,128)(2,1)} %all-gather.3.cloned.1.call-done) | data formatting | bytes 16777216
  407.5 8.4 %copy.29 = bf16[2048,2048]{1,0:T(8,128)(2,1)} copy(bf16[2048,2048]{1,0:T(8,128)(2,1)} %all-gather.5.cloned.1.call-done) | data formatting | bytes 16777216
  (3 shorter events, 0.0 us)
Async XLA Ops:
  7.2 29.1 %copy-start = (bf16[512,2048]{1,0:T(8,128)(2,1)S(1)}, bf16[512,2048]{1,0:T(8,128)(2,1)}, u32[]{:S(2)}) copy-start(bf16[512,2048]{1,0:T(8,128)(2,1)} %param.15) | copy-start | bytes 6291460
  7.2 27.1 %all-reduce.8.cloned.1.call-start = ((), (), s32[]{:S(2)}) async-start(), calls=%async_computation.3 | async-start | bytes 524288 | tf_op jit(solution)/shard_map/psum | solution.py:62
  7.2 27.1 %copy-start.2 = (bf16[512,1024]{1,0:T(8,128)(2,1)S(1)}, bf16[512,1024]{1,0:T(8,128)(2,1)}, u32[]{:S(2)}) copy-start(bf16[512,1024]{1,0:T(8,128)(2,1)} %param.13) | copy-start | bytes 3145732
  13.1 146.9 %all-reduce.6.cloned.1.call-start = ((), (), s32[]{:S(2)}) async-start(), calls=%async_computation.2 | async-start | bytes 3145728 | tf_op jit(solution)/shard_map/psum | solution.py:72
  36.3 123.7 %copy-start.4 = (f32[128,1024]{1,0:T(8,128)S(1)}, f32[128,1024]{1,0:T(8,128)}, u32[]{:S(2)}) copy-start(f32[128,1024]{1,0:T(8,128)} %param.20) | copy-start | bytes 1572868
  36.3 123.7 %copy-start.5 = (f32[128,1024]{1,0:T(8,128)S(1)}, f32[128,1024]{1,0:T(8,128)}, u32[]{:S(2)}) copy-start(f32[128,1024]{1,0:T(8,128)} %param.19) | copy-start | bytes 1572868
  38.8 247.3 %all-gather.3.cloned.1.call-start = ((), (), s32[]{:S(2)}) async-start(), calls=%async_computation | async-start | bytes 8912896 | tf_op jit(solution)/shard_map/all_gather | solution.py:92
  160.0 3.0 copy-start.3
  166.8 8.4 %copy-start.1 = (f32[128,2048]{1,0:T(8,128)}, f32[128,2048]{1,0:T(8,128)S(1)}, u32[]{:S(2)}) copy-start(f32[128,2048]{1,0:T(8,128)S(1)} %get-tuple-element.47) | copy-start | bytes 3145732
  174.5 225.3 %all-gather.5.cloned.1.call-start = ((), (), s32[]{:S(2)}) async-start(), calls=%async_computation.1 | async-start | bytes 8912896 | tf_op jit(solution)/shard_map/all_gather | solution.py:93
Sparse Core Ops, SparseCore 0:
  13.3 21.0 all-reduce.7
  41.1 118.9 all-reduce.5
  174.6 111.4 all-gather.2
  289.3 110.4 all-gather.4
where the time goes:
time: 423 us
  waiting for transfers between devices  363 us (86%)
  matrix products  18.3 us (4%)
  local copies, waits for them, and re-layouts  16.2 us (4%)
  between operations  15.2 us (4%)
  other arithmetic  6.75 us (2%)
    psum x1, waiting for transfers between devices, per_device(): lax.psum((value_partial, output_partial), 'fs')  121 us
    all_gather x1, waiting for transfers between devices, per_device(): lax.all_gather(output_new.astype(jnp.bfloat16), 'fs', axis=0, tiled=True)  114 us
    all_gather x1, waiting for transfers between devices, per_device(): lax.all_gather(value_new.astype(jnp.bfloat16), 'fs', axis=0, tiled=True)  107 us
    psum x1, waiting for transfers between devices, per_device(): lax.psum(input_partial.astype(jnp.bfloat16), 'tp').astype(jnp.float32)  21.1 us
    unnamed x14, local copies, waits for them, and re-layouts  16.2 us
  transfers between devices with their start and end apart: 4, of which 4 were waited for; matrix products, arithmetic and copies ran while one was open for 1% of the time, Pallas kernels for 0%

commit v1 on v0

v1 whole, which is shorter than its diff:
```python
import functools

import jax
import jax.numpy as jnp
from jax import lax
from jax.experimental import pallas as pl
from jax.experimental.pallas import tpu as pltpu
from jax.sharding import PartitionSpec as P

BETA_ONE = 0.8
BETA_TWO = 0.9
EPSILON = 1e-08
STEP_RATE = 0.005
FLOOR = 0.25

MESH = pl.DeviceIdType.MESH
PIECES = 8
UP, DOWN, ACROSS_A, ACROSS_B = range(4)
GROUPS = (
    (0, 0, 4, True, (ACROSS_A, ACROSS_B)),
    (1, 0, 4, True, (ACROSS_B, ACROSS_A)),
    (0, 4, 7, True, (ACROSS_B, ACROSS_A)),
    (1, 4, 7, True, (ACROSS_A, ACROSS_B)),
    (0, 7, 8, False, (ACROSS_A, ACROSS_B)),
    (1, 7, 8, False, (ACROSS_B, ACROSS_A)),
)


def transfer_kernel(
    n_fs,
    n_tp,
    input_ref,
    mixer_ref,
    value_cot_ref,
    output_cot_ref,
    value_own,
    output_own,
    value_all,
    output_all,
    value_sum,
    output_sum,
    near_in,
    near_mix,
    value_part,
    output_part,
    value_recv,
    output_recv,
    gather_send,
    gather_recv,
    local_sem,
    near_send,
    near_recv,
    scatter_send,
    scatter_recv,
    total_send,
    total_recv,
):
    me = lax.axis_index("fs")
    column = lax.axis_index("tp")
    n_a = 2 if n_fs % 2 == 0 else 1
    n_b = 2 if n_fs % 4 == 0 else 1
    plane = n_a * n_b
    n_z = n_fs // plane
    here_a = lax.rem(me, n_a)
    here_b = lax.rem(me // n_a, n_b)
    here_z = me // plane
    owns = (value_own, output_own)
    alls = (value_all, output_all)

    def index_of(z, flip_a, flip_b):
        a = n_a - 1 - here_a if flip_a else here_a
        b = n_b - 1 - here_b if flip_b else here_b
        return z * plane + b * n_a + a

    targets = {
        UP: me + plane,
        DOWN: me - plane,
        ACROSS_A: index_of(here_z, True, False),
        ACROSS_B: index_of(here_z, False, True),
    }
    can = {UP: here_z < n_z - 1, DOWN: here_z > 0, ACROSS_A: n_a > 1, ACROSS_B: n_b > 1}

    def copy_of(way, source, group, own):
        array, low, high, _, _ = GROUPS[group]
        there = alls[array].at[source, low:high]
        return pltpu.make_async_remote_copy(
            src_ref=owns[array].at[low:high] if own else there,
            dst_ref=there,
            send_sem=gather_send.at[way, source, group],
            recv_sem=gather_recv.at[source, group],
            device_id={"fs": targets[way]},
            device_id_type=MESH,
        )

    def guarded(condition, action):
        if isinstance(condition, bool):
            if condition:
                action()
        else:
            pl.when(condition)(action)

    sent = []

    def send(way, source, group, own=False, valid=True):
        def begin():
            copy_of(way, source, group, own).start()

        def finish():
            copy_of(way, source, group, own).wait_send()

        condition = can[way]
        if valid is not True:
            condition = jnp.logical_and(condition, valid) if condition is not True else valid
        guarded(condition, begin)
        sent.append((condition, finish))

    def take(way, source, group):
        copy_of(way, source, group, False).wait_recv()

    def flips(axis):
        return axis == ACROSS_A, axis == ACROSS_B

    z_groups = [g for g in range(len(GROUPS)) if GROUPS[g][3]]
    plane_groups = [g for g in range(len(GROUPS)) if not GROUPS[g][3]]

    near = []
    for k in range(1, n_tp):
        for i, (src, dst) in enumerate(((input_ref, near_in), (mixer_ref, near_mix))):
            near.append(
                pltpu.make_async_remote_copy(
                    src_ref=src,
                    dst_ref=dst.at[k - 1],
                    send_sem=near_send.at[k - 1, i],
                    recv_sem=near_recv.at[k - 1, i],
                    device_id={"tp": lax.rem(column + k, n_tp)},
                    device_id_type=MESH,
                )
            )
    for copy in near:
        copy.start()

    for group in z_groups + plane_groups:
        for way in (UP, DOWN, ACROSS_A, ACROSS_B):
            send(way, me, group, own=True)
    keep = [
        pltpu.make_async_copy(owns[i], alls[i].at[me], local_sem.at[i]) for i in range(2)
    ]
    for copy in keep:
        copy.start()

    for copy in near:
        copy.wait()
    input_total = input_ref[...].astype(jnp.float32)
    mixer_total = mixer_ref[...].astype(jnp.float32)
    for k in range(n_tp - 1):
        input_total += near_in[k].astype(jnp.float32)
        mixer_total += near_mix[k].astype(jnp.float32)
    across = (((0,), (0,)), ((), ()))
    rows = value_part.shape[1]
    scatter = []
    for i, (left, right, part, recv) in enumerate(
        (
            (input_total.astype(jnp.bfloat16), value_cot_ref, value_part, value_recv),
            (mixer_total.astype(jnp.bfloat16), output_cot_ref, output_part, output_recv),
        )
    ):
        width = right.shape[1]
        tile = 512 if width % 512 == 0 else width
        for c in range(width // tile):
            cols = slice(c * tile, (c + 1) * tile)
            product = lax.dot_general(
                left, right[:, cols], across, preferred_element_type=jnp.float32
            )
            for s in range(n_fs):
                part[s, :, cols] = product[s * rows : (s + 1) * rows]
        for k in range(1, n_fs):
            there = lax.rem(me + k, n_fs)
            copy = pltpu.make_async_remote_copy(
                src_ref=part.at[there],
                dst_ref=recv.at[k],
                send_sem=scatter_send.at[i, k],
                recv_sem=scatter_recv.at[i, k],
                device_id={"fs": there},
                device_id_type=MESH,
            )
            copy.start()
            scatter.append(copy)

    def plane_round():
        for group in plane_groups:
            first, second = GROUPS[group][4]
            if can[first]:
                source = index_of(here_z, *flips(first))
                take(first, source, group)
                for way in (second, UP, DOWN):
                    send(way, source, group)
        for group in plane_groups:
            first, second = GROUPS[group][4]
            if can[second]:
                for both in (False, True):
                    if both and not can[first]:
                        continue
                    source = index_of(
                        here_z,
                        second == ACROSS_A or (both and first == ACROSS_A),
                        second == ACROSS_B or (both and first == ACROSS_B),
                    )
                    take(second, source, group)
                    for way in (UP, DOWN):
                        send(way, source, group)

    def z_round(d):
        for sign, onward in ((-1, UP), (1, DOWN)):
            z = here_z + sign * d
            valid = z >= 0 if sign < 0 else z <= n_z - 1

            for group in z_groups:
                source = index_of(z, False, False)

                @pl.when(valid)
                def _(group=group, source=source):
                    take(DOWN if onward == UP else UP, source, group)

                send(onward, source, group, valid=valid)
                for way in GROUPS[group][4]:
                    send(way, source, group, valid=valid)
            for group in plane_groups:
                for flip_a in range(n_a):
                    for flip_b in range(n_b):
                        source = index_of(z, flip_a == 1, flip_b == 1)

                        @pl.when(valid)
                        def _(group=group, source=source):
                            take(DOWN if onward == UP else UP, source, group)

                        send(onward, source, group, valid=valid)

    def column_round(d):
        for sign in (-1, 1):
            if d == 0 and sign == 1:
                continue
            z = here_z + sign * d
            valid = True if d == 0 else (z >= 0 if sign < 0 else z <= n_z - 1)
            for group in z_groups:
                first, second = GROUPS[group][4]
                if not can[first]:
                    continue
                source = index_of(z, *flips(first))
                guarded(valid, functools.partial(take, first, source, group))
                send(second, source, group, valid=valid)

    totals = []

    def share_totals():
        for copy in scatter:
            copy.wait_recv()
        for i, (part, recv, out) in enumerate(
            ((value_part, value_recv, value_sum), (output_part, output_recv, output_sum))
        ):
            total = part[me]
            for k in range(1, n_fs):
                total += recv[k]
            out[me] = total
            for k in range(1, n_fs):
                there = lax.rem(me + k, n_fs)
                copy = pltpu.make_async_remote_copy(
                    src_ref=out.at[me],
                    dst_ref=out.at[me],
                    send_sem=total_send.at[i, k],
                    recv_sem=total_recv.at[i, k],
                    device_id={"fs": there},
                    device_id_type=MESH,
                )
                copy.start()
                source = lax.rem(me + n_fs - k, n_fs)
                arriving = pltpu.make_async_remote_copy(
                    src_ref=out.at[source],
                    dst_ref=out.at[source],
                    send_sem=total_send.at[i, k],
                    recv_sem=total_recv.at[i, k],
                    device_id={"fs": there},
                    device_id_type=MESH,
                )
                totals.append((copy, arriving))

    plane_round()
    column_round(0)
    for d in range(1, n_z):
        z_round(d)
        if d == 1:
            share_totals()
        column_round(d)
    if n_z == 1:
        share_totals()

    for group in z_groups:
        first, second = GROUPS[group][4]
        if can[second]:
            for z in range(n_z):
                for both in (False, True):
                    if both and not can[first]:
                        continue
                    source = index_of(
                        z,
                        second == ACROSS_A or (both and first == ACROSS_A),
                        second == ACROSS_B or (both and first == ACROSS_B),
                    )
                    take(second, source, group)
    for copy, arriving in totals:
        copy.wait_send()
        arriving.wait_recv()
    for copy in scatter:
        copy.wait_send()
    for condition, finish in sent:
        guarded(condition, finish)
    for copy in keep:
        copy.wait()


def transfers(n_fs, n_tp, inputs, mixer, value_cot, output_cot, value_own, output_own, rank):
    f32, bf16 = jnp.float32, jnp.bfloat16
    rows = rank // n_fs
    value_cols, output_cols = value_cot.shape[1], output_cot.shape[1]
    tokens = inputs.shape[0]
    vmem = pl.BlockSpec(memory_space=pltpu.VMEM)
    hbm = pl.BlockSpec(memory_space=pltpu.HBM)
    groups = len(GROUPS)
    dma = pltpu.SemaphoreType.DMA
    return pl.pallas_call(
        functools.partial(transfer_kernel, n_fs, n_tp),
        out_shape=(
            jax.ShapeDtypeStruct((n_fs,) + value_own.shape, bf16),
            jax.ShapeDtypeStruct((n_fs,) + output_own.shape, bf16),
            jax.ShapeDtypeStruct((n_fs, rows, value_cols), f32),
            jax.ShapeDtypeStruct((n_fs, rows, output_cols), f32),
        ),
        in_specs=[vmem] * 6,
        out_specs=(hbm, hbm, vmem, vmem),
        scratch_shapes=[
            pltpu.VMEM((max(n_tp - 1, 1), tokens, rank), bf16),
            pltpu.VMEM((max(n_tp - 1, 1), tokens, rank), bf16),
            pltpu.VMEM((n_fs, rows, value_cols), f32),
            pltpu.VMEM((n_fs, rows, output_cols), f32),
            pltpu.VMEM((n_fs, rows, value_cols), f32),
            pltpu.VMEM((n_fs, rows, output_cols), f32),
            dma((4, n_fs, groups)),
            dma((n_fs, groups)),
            dma((2,)),
            dma((max(n_tp - 1, 1), 2)),
            dma((max(n_tp - 1, 1), 2)),
            dma((2, n_fs)),
            dma((2, n_fs)),
            dma((2, n_fs)),
            dma((2, n_fs)),
        ],
        compiler_params=pltpu.CompilerParams(has_side_effects=True),
    )(inputs, mixer, value_cot, output_cot, value_own, output_own)


def moments(first, second, projected):
    first_new = BETA_ONE * first + (1.0 - BETA_ONE) * projected
    second_new = BETA_TWO * second + (1.0 - BETA_TWO) * projected * projected
    normalized = first_new / (jnp.sqrt(second_new) + EPSILON)
    return (first_new, second_new, normalized)


def halves(norm):
    high = lax.reduce_precision(norm, 8, 7)
    low = norm - high
    return jnp.concatenate([high, low], axis=0).astype(jnp.bfloat16)


def per_device(
    n_fs,
    n_tp,
    normed_input,
    value_cotangent,
    mixer_output,
    output_cotangent,
    value_factor,
    output_factor,
    value_master,
    value_moment,
    value_second,
    output_master,
    output_moment,
    output_second,
):
    row_index = lax.axis_index("fs")
    column_index = lax.axis_index("tp")
    rank = value_factor.shape[1]
    value_rows, value_cols = value_master.shape
    output_rows, output_cols = output_master.shape
    feature_cols = normed_input.shape[1]
    factor_features = lax.dynamic_slice_in_dim(
        value_factor, column_index * feature_cols, feature_cols, 0
    )
    input_partial = jnp.dot(
        normed_input, factor_features, preferred_element_type=jnp.float32
    ).astype(jnp.bfloat16)
    head_cols = mixer_output.shape[1]
    factor_heads = lax.dynamic_slice_in_dim(output_factor, column_index * head_cols, head_cols, 0)
    mixer_partial = jnp.dot(
        mixer_output, factor_heads, preferred_element_type=jnp.float32
    ).astype(jnp.bfloat16)

    value_all, output_all, value_sum, output_sum = transfers(
        n_fs,
        n_tp,
        input_partial,
        mixer_partial,
        value_cotangent,
        output_cotangent,
        value_master.astype(jnp.bfloat16).reshape(PIECES, value_rows // PIECES, value_cols),
        output_master.astype(jnp.bfloat16).reshape(PIECES, output_rows // PIECES, output_cols),
        rank,
    )
    value_moment_new, value_second_new, value_norm = moments(
        value_moment, value_second, value_sum.reshape(rank, value_cols)
    )
    output_moment_new, output_second_new, output_norm = moments(
        output_moment, output_second, output_sum.reshape(rank, output_cols)
    )
    value_total, output_total = lax.psum(
        (jnp.sum(value_norm * value_norm), jnp.sum(output_norm * output_norm)), "tp"
    )
    value_scale = lax.rsqrt(value_total / (rank * value_cols * n_tp) + FLOOR)
    output_scale = lax.rsqrt(output_total / (rank * output_cols * n_tp) + FLOOR)

    def update(factor, norm, scale, master, gathered):
        pair = halves(norm)
        double = jnp.concatenate([factor, factor], axis=1)
        rows = master.shape[0]
        double_here = lax.dynamic_slice_in_dim(double, row_index * rows, rows, 0)
        step = scale * jnp.dot(double_here, pair, preferred_element_type=jnp.float32)
        new = master - STEP_RATE * step
        full = jnp.dot(double, pair, preferred_element_type=jnp.float32)
        flat = gathered.reshape(n_fs * rows, master.shape[1]).astype(jnp.float32)
        copy = (flat - (STEP_RATE * scale) * full).astype(jnp.bfloat16)
        return step, new, copy

    value_step, value_new, value_copy = update(
        value_factor, value_norm, value_scale, value_master, value_all
    )
    output_step, output_new, output_copy = update(
        output_factor, output_norm, output_scale, output_master, output_all
    )
    return (
        value_step,
        value_new,
        value_copy,
        value_moment_new,
        value_second_new,
        output_step,
        output_new,
        output_copy,
        output_moment_new,
        output_second_new,
    )


def solution(mesh):
    return jax.shard_map(
        functools.partial(per_device, mesh.shape["fs"], mesh.shape["tp"]),
        mesh=mesh,
        in_specs=(
            P("fs", "tp"),
            P("fs", "tp"),
            P("fs", "tp"),
            P("fs", "tp"),
            P(),
            P(),
            P("fs", "tp"),
            P(None, "tp"),
            P(None, "tp"),
            P("fs", "tp"),
            P(None, "tp"),
            P(None, "tp"),
        ),
        out_specs=(
            P("fs", "tp"),
            P("fs", "tp"),
            P(None, "tp"),
            P(None, "tp"),
            P(None, "tp"),
            P("fs", "tp"),
            P("fs", "tp"),
            P(None, "tp"),
            P(None, "tp"),
            P(None, "tp"),
        ),
        check_vma=False,
    )
```

time: 423 us -> 225 us (0.53)
  waiting for transfers between devices: 363 us -> 0 us
  Pallas kernels: 0 us -> 178 us
  between operations: 15.2 us -> 2.29 us
  local copies, waits for them, and re-layouts: 16.2 us -> 6.47 us
  matrix products: 18.3 us -> 24.4 us
    all_gather x2 -> x0, waiting for transfers between devices: 220 us -> none  [the longest x1 114 us: per_device(): lax.all_gather(output_new.astype(jnp.bfloat16), 'fs', axis=0, tiled=True)]
    pallas_call x0 -> x1, Pallas kernels: none -> 178 us  [transfers(): pl.pallas_call(functools.partial(transfer_kernel, n_fs, n_tp), out_shape=...]
    psum x2 -> x0, waiting for transfers between devices: 142 us -> none  [the longest x1 121 us: per_device(): lax.psum((value_partial, output_partial), 'fs')]
    unnamed x14 -> x26, local copies, waits for them, and re-layouts: 16.2 us -> 5.05 us
    another operation x0 -> x4, other arithmetic: none -> 7.39 us
    dot_general x4, matrix products: 12.5 us -> 19.4 us  [the longest x2 13.9 us: update(): full = jnp.dot(double, pair, preferred_element_type=jnp.float32)]
    reduce_sum x2 -> x0, other arithmetic: 6.75 us -> none  [the longest x1 3.74 us: per_device(): jnp.sum(output_norm * output_norm)]
  transfers between devices with their start and end apart: 4 -> 0, of which waited for: 4 -> 0; matrix products, arithmetic and copies ran while one was open for 1% -> 0% of each run, Pallas kernels for 0% -> 0%
where the time goes in v1:
time: 225 us; the launch traced here: 224 us
  Pallas kernels  178 us (79%)
  matrix products  24.4 us (11%)
  other arithmetic  10.3 us (5%)
  local copies, waits for them, and re-layouts  6.47 us (3%)
  blocking collectives  3.16 us (1%)
  between operations  2.29 us (1%)
    pallas_call x1, Pallas kernels, transfers(): pl.pallas_call(functools.partial(transfer_kernel, n_fs, n_tp), out_shape=...  178 us
    dot_general x2, matrix products, update(): full = jnp.dot(double, pair, preferred_element_type=jnp.float32)  13.9 us
    another operation x4, other arithmetic  7.39 us
    dot_general x2, matrix products, update(): jnp.dot(double_here, pair, preferred_element_type=jnp.float32)  5.51 us
    unnamed x26, local copies, waits for them, and re-layouts  5.05 us

profile of v1, /device:TPU:0, one launch (start us, length us, event | category | flops | bytes accessed | tf_op | source)
XLA Modules:
  0.0 224.4 jit_solution(16621076342794427241)
XLA Ops:
  0.6 0.0 copy-start
  0.7 2.5 %fusion.3.mixer_ref = bf16[512,128]{1,0:T(8,128)(2,1)} fusion(bf16[512,1024]{1,0:T(8,128)(2,1)} %param.14, bf16[2048,128]{1,0:T(8,128)(2,1)} %param.17, s32[]{:T(128)S(6)} %select_n.13), kind=kOutput, calls=%fused_computation.12 | convolution fusion | flops 134283264 | bytes 1441796 | tf_op jit(solution)/shard_map/dot_general | solution.py:403
  3.2 0.0 copy-done
  3.2 2.5 %fusion.2.input_ref = bf16[512,128]{1,0:T(8,128)(2,1)} fusion(bf16[512,2048]{1,0:T(8,128)(2,1)S(1)} %copy-done, bf16[4096,128]{1,0:T(8,128)(2,1)} %param.16, s32[]{:T(128)S(6)} %select_n.12), kind=kOutput, calls=%fused_computation.11 | convolution fusion | flops 268500992 | bytes 2752516 | tf_op jit(solution)/shard_map/dot_general | solution.py:398
  5.7 2.1 convert_element_type.40
  7.8 0.0 copy-done.1
  7.8 0.9 convert_element_type.41
  8.6 177.7 %shard_map.195 = (bf16[16,8,32,1024]{3,2,1,0:T(8,128)(2,1)}, bf16[16,8,16,2048]{3,2,1,0:T(8,128)(2,1)}, f32[16,8,1024]{2,1,0:T(8,128)}, f32[16,8,2048]{2,1,0:T(8,128)}) custom-call(bf16[512,128]{1,0:T(8,128)(2,1)} %fusion.2.input_ref, bf16[512,128]{1,0:T(8,128)(2,1)} %fusion.3.mixer_ref, bf16[512,1024]{1,0:T(8,128)(2,1)} %value_cot_ref.1, ...), custom_call_target="tpu_custom_call" | custom-call | tf_op jit(solution)/shard_map/pallas_call | solution.py:329
  186.3 0.0 copy-start.8
  186.3 0.0 copy-start.9
  186.3 0.0 copy-start.10
  186.4 3.8 %reduce-precision_convert_fusion = (bf16[128,2048]{1,0:T(8,128)(2,1)}, f32[128,2048]{1,0:T(8,128)S(1)}, f32[128,2048]{1,0:T(8,128)}, f32[128,2048]{1,0:T(8,128)}) fusion(f32[16,8,2048]{2,1,0:T(8,128)} %get-tuple-element.16, f32[128,2048]{1,0:T(8,128)} %param.23, f32[128,2048]{1,0:T(8,128)} %param.22), kind=kLoop, calls=%fused_computation.7 | loop fusion | flops 2883584 | bytes 6815744 | tf_op jit(solution)/shard_map/convert.2
  190.2 1.6 fusion.4
  191.8 0.0 copy-done.10
  191.8 1.2 reduce-precision_convert_fusion.1
  193.0 0.7 fusion.7
  193.8 3.2 %all-reduce = (f32[]{:T(128)}, f32[]{:T(128)}) all-reduce(f32[]{:T(128)} %get-tuple-element.31, f32[]{:T(128)} %get-tuple-element.29), channel_id=1, replica_groups=mesh['fs'=16,'tp'=2] {'tp'}, use_global_device_ids=true, to_apply=%region_1.0 | all-reduce | flops 2 | bytes 16 | tf_op jit(solution)/shard_map/psum | solution.py:424
  197.6 0.0 copy-start.4
  197.6 0.0 copy-start.5
  197.6 1.2 constant_dynamic-update-slice_fusion.3
  198.9 1.2 constant_dynamic-update-slice_fusion.2
  200.0 0.0 copy-start.11
  200.0 1.0 copy-done.11
  201.0 6.9 %fusion = bf16[2048,2048]{1,0:T(8,128)(2,1)} fusion(bf16[2048,2048]{1,0:T(8,128)(2,1)} %bitcast.31, bf16[2048,256]{1,0:T(8,128)(2,1)S(1)} %constant_dynamic-update-slice_fusion.2, f32[]{:T(128)S(6)} %mul.149, bf16[128,2048]{1,0:T(8,128)(2,1)S(1)} %copy-done.4, bf16[128,2048]{1,0:T(8,128)(2,1)S(1)} %copy-done.5), kind=kOutput, calls=%fused_computation.1 | convolution fusion | flops 2166358016 | bytes 18874372 | tf_op jit(solution)/shard_map/dot_general | solution.py:437
  207.9 2.9 %multiply_subtract_fusion = (f32[128,2048]{1,0:T(8,128)}, f32[128,2048]{1,0:T(8,128)}) fusion(f32[128,2048]{1,0:T(8,128)S(1)} %copy-done.1, bf16[128,2048]{1,0:T(8,128)(2,1)} %get-tuple-element.28, bf16[128,2048]{1,0:T(8,128)(2,1)} %get-tuple-element.20, bf16[2048,256]{1,0:T(8,128)(2,1)} %copy-done.11, s32[]{:T(128)S(6)} %select_n.15, f32[]{:T(128)S(6)} %rsqrt.7), kind=kOutput, calls=%fused_computation.18 | convolution fusion | flops 137101312 | bytes 4259848 | tf_op jit(solution)/shard_map/dot_general | solution.py:435
  211.7 1.4 constant_dynamic-update-slice_fusion.1
  213.1 0.2 constant_dynamic-update-slice_fusion
  213.4 0.0 copy-start.7
  213.4 1.4 copy-done.7
  214.7 0.0 copy-done.6
  214.8 7.0 %fusion.1 = bf16[4096,1024]{1,0:T(8,128)(2,1)} fusion(bf16[4096,1024]{1,0:T(8,128)(2,1)} %bitcast.30, bf16[4096,256]{1,0:T(8,128)(2,1)S(1)} %constant_dynamic-update-slice_fusion, f32[]{:T(128)S(6)} %mul.131, bf16[128,1024]{1,0:T(8,128)(2,1)S(1)} %get-tuple-element.30, bf16[128,1024]{1,0:T(8,128)(2,1)S(1)} %copy-done.6), kind=kOutput, calls=%fused_computation.3 | convolution fusion | flops 2165309440 | bytes 19398660 | tf_op jit(solution)/shard_map/dot_general | solution.py:437
  221.7 2.6 %multiply_subtract_fusion.1 = (f32[256,1024]{1,0:T(8,128)}, f32[256,1024]{1,0:T(8,128)}) fusion(f32[256,1024]{1,0:T(8,128)S(1)} %copy-done.3, bf16[128,1024]{1,0:T(8,128)(2,1)S(1)} %get-tuple-element.30, bf16[128,1024]{1,0:T(8,128)(2,1)} %get-tuple-element.24, bf16[4096,256]{1,0:T(8,128)(2,1)} %copy-done.7, s32[]{:T(128)S(6)} %select_n.14, f32[]{:T(128)S(6)} %rsqrt.6), kind=kOutput, calls=%fused_computation.21 | convolution fusion | flops 136052736 | bytes 3801096 | tf_op jit(solution)/shard_map/dot_general | solution.py:435
  (10 shorter events, 0.0 us)
Async XLA Ops:
  0.6 2.5 %copy-start = (bf16[512,2048]{1,0:T(8,128)(2,1)S(1)}, bf16[512,2048]{1,0:T(8,128)(2,1)}, u32[]{:S(2)}) copy-start(bf16[512,2048]{1,0:T(8,128)(2,1)} %param.12) | copy-start | bytes 6291460
  3.2 4.6 %copy-start.1 = (f32[128,2048]{1,0:T(8,128)S(1)}, f32[128,2048]{1,0:T(8,128)}, u32[]{:S(2)}) copy-start(f32[128,2048]{1,0:T(8,128)} %param.21) | copy-start | bytes 3145732
  186.3 5.5 %copy-start.8 = (f32[128,1024]{1,0:T(8,128)S(1)}, f32[128,1024]{1,0:T(8,128)}, u32[]{:S(2)}) copy-start(f32[128,1024]{1,0:T(8,128)} %param.20) | copy-start | bytes 1572868
  186.3 5.5 %copy-start.9 = (f32[128,1024]{1,0:T(8,128)S(1)}, f32[128,1024]{1,0:T(8,128)}, u32[]{:S(2)}) copy-start(f32[128,1024]{1,0:T(8,128)} %param.19) | copy-start | bytes 1572868
  186.3 5.5 %copy-start.10 = (f32[16,8,1024]{2,1,0:T(8,128)S(1)}, f32[16,8,1024]{2,1,0:T(8,128)}, u32[]{:S(2)}) copy-start(f32[16,8,1024]{2,1,0:T(8,128)} %get-tuple-element.14) | copy-start | bytes 1572868
  197.6 3.4 %copy-start.4 = (bf16[128,2048]{1,0:T(8,128)(2,1)S(1)}, bf16[128,2048]{1,0:T(8,128)(2,1)}, u32[]{:S(2)}) copy-start(bf16[128,2048]{1,0:T(8,128)(2,1)} %get-tuple-element.28) | copy-start | bytes 1572868
  197.6 3.4 %copy-start.5 = (bf16[128,2048]{1,0:T(8,128)(2,1)S(1)}, bf16[128,2048]{1,0:T(8,128)(2,1)}, u32[]{:S(2)}) copy-start(bf16[128,2048]{1,0:T(8,128)(2,1)} %get-tuple-element.20) | copy-start | bytes 1572868
  200.0 1.0 copy-start.11
  210.8 2.3 %copy-start.2 = (bf16[4096,128]{1,0:T(8,128)(2,1)S(1)}, bf16[4096,128]{1,0:T(8,128)(2,1)}, u32[]{:S(2)}) copy-start(bf16[4096,128]{1,0:T(8,128)(2,1)} %param.16) | copy-start | bytes 3145732
  211.6 3.1 %copy-start.6 = (bf16[128,1024]{1,0:T(8,128)(2,1)S(1)}, bf16[128,1024]{1,0:T(8,128)(2,1)}, u32[]{:S(2)}) copy-start(bf16[128,1024]{1,0:T(8,128)(2,1)} %get-tuple-element.24) | copy-start | bytes 786436
  213.4 1.4 copy-start.7
  214.7 7.0 %copy-start.3 = (f32[256,1024]{1,0:T(8,128)S(1)}, f32[256,1024]{1,0:T(8,128)}, u32[]{:S(2)}) copy-start(f32[256,1024]{1,0:T(8,128)} %param.18) | copy-start | bytes 3145732
